TPU v7x, 128 devices: a whole 4x4x4 slice. The times are simulated.
128 devices in a mesh: ep: 32 (over z, y, core), tp: 4 (over x).
Axes of the slice: x: 4, y: 4, z: 4, core: 2. Of those that a mesh axis runs over, the one named last changes fastest.
Arguments:
- value_in: bfloat16 [16384, 1024], P('ep', 'tp'), may hold values from -6 to 6
- gate_in: bfloat16 [16384, 1024], P('ep', 'tp'), may hold values from -6 to 6
- outer_gate: bfloat16 [16384, 1024], P('ep', 'tp'), may hold values from -6 to 6
- conv_weight: bfloat16 [3, 1024], P(None, 'tp'), may hold values from -3.5 to 3.5
- out_weight: bfloat16 [1024, 2048], P('tp'), may hold values from -0.1875 to 0.1875
- moe_tokens: bfloat16 [16384, 2048], P(('ep', 'tp')), may hold values from -6 to 6
- norm_gain: bfloat16 [2048], replicated, may hold values from 0.099609375 to 1.8984375
- routes: int32 [16384, 2], P(('ep', 'tp')), may hold values from 0 to 31, all different within a row; in each aligned block of 128 rows (0 to 127, 128 to 255, ...) at most 12 rows name the same one
- route_weight: float32 [16384, 2], P(('ep', 'tp')), may hold values from 0.1 to 1
- expert_gate: bfloat16 [32, 2048, 6144], P('ep', None, 'tp'), may hold values from -0.125 to 0.125
- expert_up: bfloat16 [32, 2048, 6144], P('ep', None, 'tp'), may hold values from -0.125 to 0.125
- expert_down: bfloat16 [32, 6144, 2048], P('ep', 'tp'), may hold values from -0.078125 to 0.078125
Outputs:
- mixer_out: bfloat16 [16384, 2048], P(('ep', 'tp'))
- moe_out: bfloat16 [16384, 2048], P(('ep', 'tp'))
Inputs may be any that keep to these rules, and one draw needn't show every extreme that they name: `routes`: each row names 2 different experts. Among the rows of one device no expert is named by more than 12 rows, a bound that some blocks reach.
All inputs are finite; a program needn't handle non-finite values.
Results may differ from a plain program's by a relative error of at most 0.012.
Values may be sent and summed in bfloat16 or wider, within the bound.
No kernel may reach another device: no remote copies, remote signals or barrier semaphores. Data moves between devices by JAX's collectives and lax.ppermute only.
A program may use at most 128 MiB of HBM per device.

v0:
```python
import jax
import jax.numpy as jnp
from jax import lax
from jax.sharding import Mesh
from jax.sharding import PartitionSpec as P

EP = ("ep_0", "ep_1", "ep_2")
EP_TP = ("ep_0", "ep_1", "ep_2", "tp")


def extended(x, sides, width):
    for axis, dim in sides:
        size, length = (lax.axis_size(axis), x.shape[dim])
        up = [(i, (i + 1) % size) for i in range(size - 1)]
        down = [(j, i) for i, j in up]
        last = lax.slice_in_dim(x, length - width, length, axis=dim)
        leading = lax.slice_in_dim(x, 0, width, axis=dim)
        before = lax.ppermute(last, axis, up)
        after = lax.ppermute(leading, axis, down)
        x = jnp.concatenate([before, x, after], axis=dim)
    return x


def in_order(parts, dim):
    lengths = list(parts.shape[1:])
    lengths[dim] *= parts.shape[0]
    return jnp.moveaxis(parts, 0, dim).reshape(lengths)


def on_gathered_pieces(x, axis, dim, apply, out_dim):
    size, width = (lax.axis_size(axis), x.shape[dim])
    count = 2 if width % 2 == 0 else 1
    done, length = ([], width // count)
    for k in range(count):
        slab = lax.slice_in_dim(x, k * length, (k + 1) * length, axis=dim)
        starts = jnp.arange(size) * width + k * length
        done.append(jax.vmap(apply)(lax.all_gather(slab, axis), starts))
    return in_order(jnp.concatenate(done, axis=out_dim + 1), out_dim)


def in_blocks(x, dim, length):
    before, after = (x.shape[:dim], x.shape[dim + 1 :])
    return jnp.moveaxis(x.reshape(*before, length, -1, *after), dim, 0)


def exchange_in_order(parts, axes, turns):
    inside = parts.shape[1:]
    whole = parts.reshape(*(lax.axis_size(a) for a in axes), *inside)
    for k in turns:
        whole = lax.all_to_all(whole, axes[k], k, k, tiled=True)
    return whole.reshape(-1, *inside)


def two_step_exchange(x, groups, turns, split_dim, concat_dim):
    length = lax.axis_size(groups[0]) * lax.axis_size(groups[1])
    parts = in_blocks(x, split_dim, length)
    return in_order(exchange_in_order(parts, groups, turns), concat_dim)


def rounded(values):
    return lax.optimization_barrier(values.astype(jnp.bfloat16)).astype(jnp.float32)


def mixer_half(value_in, gate_in, outer_gate, conv_weight, out_weight):
    product = (value_in.astype(jnp.float32) * gate_in.astype(jnp.float32)).astype(jnp.bfloat16)
    padded = extended(product, ((EP, 0),), 1).astype(jnp.float32)
    taps = conv_weight.astype(jnp.float32)
    convolved = padded[:-2] * taps[0] + padded[1:-1] * taps[1] + padded[2:] * taps[2]
    mixed_rows = (outer_gate.astype(jnp.float32) * convolved).astype(jnp.bfloat16)
    return lax.psum_scatter(
        rounded(jnp.dot(mixed_rows, out_weight, preferred_element_type=jnp.float32)).astype(
            jnp.bfloat16
        ),
        "tp",
        scatter_dimension=0,
        tiled=True,
    )


def expert_half(moe_tokens, norm_gain, routes, route_weight, expert_gate, expert_up, expert_down):
    row_total, top_count = routes.shape
    features = moe_tokens.shape[1]
    local_units = expert_gate.shape[2]
    experts = lax.axis_size(EP)
    capacity = 3 * top_count * row_total // (2 * experts)
    tokens_f32 = moe_tokens.astype(jnp.float32)
    normed = (
        tokens_f32
        * lax.rsqrt(jnp.mean(tokens_f32 * tokens_f32, axis=-1, keepdims=True) + 1e-06)
        * norm_gain.astype(jnp.float32)
    ).astype(jnp.bfloat16)
    flat_ids = routes.reshape(row_total * top_count)
    matches = (flat_ids[:, None] == jnp.arange(experts, dtype=jnp.int32)[None, :]).astype(jnp.int32)
    position = jnp.sum((jnp.cumsum(matches, axis=0) - 1) * matches, axis=1)
    slot_ids = flat_ids * capacity + position
    placement = slot_ids[:, None] == jnp.arange(experts * capacity, dtype=jnp.int32)[None, :]
    placement = (
        placement.reshape(row_total, top_count, experts * capacity).sum(axis=1).astype(jnp.bfloat16)
    )
    outgoing = jnp.einsum("rs,rd->sd", placement, normed, preferred_element_type=jnp.float32)
    outgoing = outgoing.astype(jnp.bfloat16).reshape(experts, capacity, features)

    def hidden_of(slot_block):
        lead = slot_block.shape[:-1]
        flat_rows = slot_block.reshape(-1, features)
        gate_act = jnp.dot(flat_rows, expert_gate[0], preferred_element_type=jnp.float32)
        up_act = jnp.dot(flat_rows, expert_up[0], preferred_element_type=jnp.float32)
        return (jax.nn.silu(gate_act) * up_act).astype(jnp.bfloat16).reshape(lead + (local_units,))

    arrived = lax.all_to_all(outgoing, EP, split_axis=0, concat_axis=0, tiled=True)

    def lift_rows(shard_piece, first_index):
        return hidden_of(shard_piece)

    hidden = on_gathered_pieces(arrived[:, None], "tp", 1, lift_rows, 1)
    group_rows = experts * capacity
    group_count = group_rows * lax.axis_size("tp") // group_rows
    selected = hidden
    selected = jnp.swapaxes(selected, 0, 1).reshape(group_count * group_rows, local_units)
    summed_back = lax.psum_scatter(
        rounded(jnp.dot(selected, expert_down[0], preferred_element_type=jnp.float32)).astype(
            jnp.bfloat16
        ),
        "tp",
        scatter_dimension=0,
        tiled=True,
    )
    returned = two_step_exchange(
        summed_back.reshape(experts, capacity, features), (("ep_0", "ep_1"), "ep_2"), (0, 1), 0, 0
    )
    picked = returned.reshape(group_rows, features)[slot_ids].reshape(
        row_total, top_count, features
    )
    return jnp.sum(route_weight[..., None] * picked.astype(jnp.float32), axis=1).astype(
        jnp.bfloat16
    )


def body(
    value_in,
    gate_in,
    outer_gate,
    conv_weight,
    out_weight,
    moe_tokens,
    norm_gain,
    routes,
    route_weight,
    expert_gate,
    expert_up,
    expert_down,
):
    mixer_out = mixer_half(value_in, gate_in, outer_gate, conv_weight, out_weight)
    moe_out = expert_half(
        moe_tokens, norm_gain, routes, route_weight, expert_gate, expert_up, expert_down
    )
    return (mixer_out, moe_out)


def solution(mesh):
    torus = Mesh(mesh.devices.reshape(4, 4, 2, mesh.shape["tp"]), ("ep_0", "ep_1", "ep_2", "tp"))
    placed = (
        P(EP, "tp"),
        P(EP, "tp"),
        P(EP, "tp"),
        P(None, "tp"),
        P("tp", None),
        P(EP_TP, None),
        P(),
        P(EP_TP, None),
        P(EP_TP, None),
        P(EP, None, "tp"),
        P(EP, None, "tp"),
        P(EP, "tp", None),
    )
    return jax.shard_map(
        body,
        mesh=torus,
        in_specs=placed,
        out_specs=(P(EP_TP, None), P(EP_TP, None)),
        check_vma=False,
    )
```

profile of v0, /device:TPU:1, one launch (start us, length us, event | category | flops | bytes accessed | tf_op | source)
XLA Modules:
  0.0 329.0 jit_solution(15447769482865396098)
XLA Ops:
  7.2 0.0 copy-start
  7.2 0.0 all-gather.3.cloned.1.call-start
  7.2 0.9 copy.36
  8.1 0.1 eq.43
  8.2 0.1 eq.39
  8.4 0.6 reduce-window.6
  9.0 0.2 slice_reduce_fusion
  9.2 0.1 fusion.20
  9.3 0.1 reduce_sum.41
  9.5 0.1 copy.40
  9.5 0.1 convert_reduce_fusion
  9.7 0.7 convert_element_type.78
  10.4 1.2 fusion.4
  11.6 2.9 convolution_convert_fusion.2
  14.5 2.4 reshape.95
  16.8 37.7 %all_to_all.15 = bf16[32,12,2048]{2,1,0:T(8,128)(2,1)S(1)} all-to-all(bf16[32,12,2048]{2,1,0:T(8,128)(2,1)S(1)} %reshape.95), channel_id=1, replica_groups=mesh['ep_0'=4,'ep_1'=4,'ep_2'=2,'tp'=4] {'ep_0','ep_1','ep_2'}, dimensions={0} | all-to-all | bytes 3145728 | tf_op jit(solution)/shard_map/all_to_all | solution.py:110
  54.5 2.0 copy.41
  56.5 0.0 all-gather.3.cloned.1.call-update
  56.6 0.0 reduce-scatter.5.cloned.1.call-start
  56.6 63.0 %all-gather.3.cloned.1.call-done = bf16[128,12,2048]{2,0,1:T(8,128)(2,1)} async-done(((bf16[32,12,2048]{2,0,1:T(8,128)(2,1)}), bf16[128,12,2048]{2,0,1:T(8,128)(2,1)}) %all-gather.3.cloned.1.call-update) | async-done | bytes 6291472 | tf_op jit(solution)/shard_map/all_gather | solution.py:37
  119.6 9.6 %copy.42 = bf16[128,12,2048]{2,1,0:T(8,128)(2,1)} copy(bf16[128,12,2048]{2,0,1:T(8,128)(2,1)} %all-gather.3.cloned.1.call-done) | data formatting | bytes 12582912 | tf_op jit(solution)/shard_map/all_gather | solution.py:37
  129.3 0.0 slice-start
  129.3 10.9 %reshape.96 = bf16[4,384,2048]{2,1,0:T(8,128)(2,1)} reshape(bf16[128,12,2048]{2,1,0:T(8,128)(2,1)} %copy.42) | data formatting | bytes 12582912 | tf_op jit(solution)/shard_map/vmap()/reshape | solution.py:105
  140.1 0.0 copy-start.1
  140.1 15.7 %fusion.1 = f32[4,384,1536]{2,1,0:T(8,128)} fusion(bf16[4,384,2048]{2,1,0:T(8,128)(2,1)} %reshape.96, bf16[1,2048,1536]{2,1,0:T(8,128)(2,1)} %param.22), kind=kOutput, calls=%fused_computation.4 | convolution fusion | flops 9663676416 | bytes 22020096 | tf_op jit(solution)/shard_map/vmap()/dot_general | solution.py:107
  155.8 0.0 slice-done
  155.8 0.0 copy-done.1
  155.8 0.0 slice-done.1
  155.8 14.2 %multiply_convert_fusion = bf16[4,384,1536]{2,1,0:T(8,128)(2,1)S(1)} fusion(f32[4,384,1536]{2,1,0:T(8,128)} %fusion.1, bf16[4,384,2048]{2,1,0:T(8,128)(2,1)S(1)} %copy-done.1, bf16[1,2048,1536]{2,1,0:T(8,128)(2,1)S(1)} %bitcast.51), kind=kOutput, calls=%fused_computation.1 | convolution fusion | flops 9677832192 | bytes 26738688 | tf_op jit(solution)/shard_map/vmap()/dot_general | solution.py:106
  170.1 3.6 %copy.43 = bf16[4,384,1536]{2,0,1:T(4,128)(2,1)S(1)} copy(bf16[4,384,1536]{2,1,0:T(8,128)(2,1)S(1)} %multiply_convert_fusion) | data formatting | bytes 9437184 | tf_op jit(solution)/shard_map/vmap()/convert_element_type | solution.py:108
  173.7 4.0 %copy.44 = bf16[4,32,12,1536]{3,2,1,0:T(8,128)(2,1)} copy(bf16[4,32,12,1536]{3,0,2,1:T(4,128)(2,1)S(1)} %bitcast.44) | data formatting | bytes 9437184 | tf_op jit(solution)/shard_map/transpose | solution.py:119
  177.8 8.2 %reshape.99 = bf16[1536,1536]{1,0:T(8,128)(2,1)} reshape(bf16[4,32,12,1536]{3,2,1,0:T(8,128)(2,1)} %copy.44) | data formatting | bytes 9437184 | tf_op jit(solution)/shard_map/reshape | solution.py:119
  186.0 15.2 %convolution_convert_fusion = bf16[1536,2048]{1,0:T(8,128)(2,1)} fusion(bf16[1536,1536]{1,0:T(8,128)(2,1)} %reshape.99, bf16[1,1536,2048]{2,1,0:T(8,128)(2,1)} %param.23), kind=kOutput, calls=%fused_computation.2 | convolution fusion | flops 9666822144 | bytes 17301504 | tf_op jit(solution)/shard_map/dot_general | solution.py:121
  201.2 0.0 copy-start.4
  201.2 0.0 reduce-scatter.5.cloned.1.call-update
  201.2 0.0 reduce-scatter.3.cloned.1.call-start
  201.3 0.9 copy-done.2
  202.1 0.1 copy-done.3
  202.2 0.1 multiply_convert_fusion.1
  202.3 3.8 %collective-permute-start = (bf16[1,256]{1,0:T(2,128)(2,1)S(1)}, bf16[1,256]{1,0:T(2,128)(2,1)S(1)}, u32[]{:S(2)}, u32[]{:S(2)}) collective-permute-start(bf16[1,256]{1,0:T(2,128)(2,1)S(1)} %get-tuple-element.2), channel_id=1, source_target_pairs={{0,4},{4,8},{8,12},{12,16},{16,20},{20,24},{24,28},{28,32},{32,36}... | collective-permute-start | bytes 1544 | tf_op jit(solution)/shard_map/ppermute | solution.py:18
  206.1 1.9 collective-permute-start.1
  208.1 0.0 copy-done.5
  208.1 0.0 collective-permute-done
  208.1 2.9 collective-permute-done.1
  211.0 0.1 maximum_convert_fusion
  211.1 0.0 copy-done
  211.1 0.0 copy-done.4
  211.1 2.2 convolution_convert_fusion.1
  213.3 0.0 reduce-scatter.3.cloned.1.call-update
  213.3 52.8 %reduce-scatter.5.cloned.1.call-done = bf16[384,2048]{1,0:T(8,128)(2,1)} async-done(((bf16[1536,2048]{1,0:T(8,128)(2,1)}), bf16[384,2048]{1,0:T(8,128)(2,1)}) %reduce-scatter.5.cloned.1.call-update) | async-done | bytes 1572880 | tf_op jit(solution)/shard_map/reduce_scatter | solution.py:120
  266.1 2.4 reshape_reshape_reshape.6
  268.5 2.8 copy.45
  271.3 6.7 %all-to-all-start.1 = ((bf16[16,2,1,12,2048]{4,1,3,2,0:T(2,128)(2,1)}), bf16[16,2,1,12,2048]{4,1,3,2,0:T(2,128)(2,1)S(1)}, u32[]{:S(2)}, u32[]{:S(2)}) async-start(bf16[16,2,1,12,2048]{4,1,3,2,0:T(2,128)(2,1)} %copy.45), calls=%async_computation.3 | async-start | bytes 3145728 | tf_op jit(solution)/shard_map/all_to_all | solution.py:50
  278.0 0.1 mul.114
  278.1 0.0 copy-done.6
  278.1 0.1 copy.35
  278.2 22.6 %all-to-all-done.1 = bf16[16,2,1,12,2048]{4,1,3,2,0:T(2,128)(2,1)S(1)} async-done(((bf16[16,2,1,12,2048]{4,1,3,2,0:T(2,128)(2,1)}), bf16[16,2,1,12,2048]{4,1,3,2,0:T(2,128)(2,1)S(1)}, u32[]{:S(2)}, u32[]{:S(2)}) %all-to-all-start.1) | async-done | bytes 1572896 | tf_op jit(solution)/shard_map/all_to_all | solution.py:50
  300.9 0.9 copy.46
  301.8 7.3 %all_to_all.16 = bf16[16,2,1,12,2048]{4,0,3,2,1:T(8,128)(2,1)S(1)} all-to-all(bf16[16,2,1,12,2048]{4,0,3,2,1:T(8,128)(2,1)S(1)} %copy.46), channel_id=1, replica_groups=mesh['ep_0'=4,'ep_1'=4,'ep_2'=2,'tp'=4] {'ep_2'}, dimensions={1} | all-to-all | bytes 3145728 | tf_op jit(solution)/shard_map/all_to_all | solution.py:50
  309.0 2.2 copy.47
  311.3 2.5 reshape_reshape_reshape.7
  313.8 2.3 gather_fusion
  316.1 2.4 reshape.100
  318.5 3.9 %multiply_reduce_fusion = bf16[128,2048]{1,0:T(8,128)(2,1)} fusion(f32[128,2,2048]{2,1,0:T(2,128)S(1)} %reshape.100, f32[128,2]{1,0:T(8,128)S(1)} %copy.35), kind=kLoop, calls=%fused_computation.9 | loop fusion | flops 786432 | bytes 2622464 | tf_op jit(solution)/shard_map/reduce_sum | solution.py:134
  (16 shorter events, 0.1 us)
Async XLA Ops:
  7.2 203.9 %copy-start = (bf16[256,2048]{1,0:T(8,128)(2,1)S(1)}, bf16[256,2048]{1,0:T(8,128)(2,1)}, u32[]{:S(2)}) copy-start(bf16[256,2048]{1,0:T(8,128)(2,1)} %param.16) | copy-start | bytes 3145732
  7.2 112.4 %all-gather.3.cloned.1.call-start = ((), (), s32[]{:S(2)}) async-start(), calls=%async_computation.7 | async-start | bytes 7864320 | tf_op jit(solution)/shard_map/all_gather | solution.py:37
  56.6 209.5 %reduce-scatter.5.cloned.1.call-start = ((), (), s32[]{:S(2)}) async-start(), calls=%async_computation.6 | async-start | bytes 7864320 | tf_op jit(solution)/shard_map/reduce_scatter | solution.py:120
  129.3 26.6 %slice-start = ((s8[6291456]{0:T(1024)(128)(4,1)}), s8[2097152]{0:T(1024)(128)(4,1)S(1)}, s32[]{:S(2)}) async-start(s8[6291456]{0:T(1024)(128)(4,1)} %bitcast.50), calls=%async_computation.8 | async-start | bytes 4194304
  140.1 15.7 %copy-start.1 = (bf16[4,384,2048]{2,1,0:T(8,128)(2,1)S(1)}, bf16[4,384,2048]{2,1,0:T(8,128)(2,1)}, u32[]{:S(2)}) copy-start(bf16[4,384,2048]{2,1,0:T(8,128)(2,1)} %reshape.96) | copy-start | bytes 18874372
  140.1 15.7 %slice-start.1 = ((s8[6291456]{0:T(1024)(128)(4,1)}), s8[4194304]{0:T(1024)(128)(4,1)S(1)}, s32[]{:S(2)}) async-start(s8[6291456]{0:T(1024)(128)(4,1)} %bitcast.50), calls=%async_computation.9 | async-start | bytes 8388608
  201.2 0.9 copy-start.2
  201.2 1.0 copy-start.3
  201.2 6.9 %copy-start.5 = (bf16[3,256]{1,0:T(4,128)(2,1)S(1)}, bf16[3,256]{1,0:T(4,128)(2,1)}, u32[]{:S(2)}) copy-start(bf16[3,256]{1,0:T(4,128)(2,1)} %param.15) | copy-start | bytes 4612
  201.2 9.9 %copy-start.4 = (bf16[512,256]{1,0:T(8,128)(2,1)S(1)}, bf16[512,256]{1,0:T(8,128)(2,1)}, u32[]{:S(2)}) copy-start(bf16[512,256]{1,0:T(8,128)(2,1)} %param.14) | copy-start | bytes 786436
  201.2 121.2 %reduce-scatter.3.cloned.1.call-start = ((), (), s32[]{:S(2)}) async-start(), calls=%async_computation.5 | async-start | bytes 2621440 | tf_op jit(solution)/shard_map/reduce_scatter | solution.py:70
  202.3 5.8 %collective-permute-start = (bf16[1,256]{1,0:T(2,128)(2,1)S(1)}, bf16[1,256]{1,0:T(2,128)(2,1)S(1)}, u32[]{:S(2)}, u32[]{:S(2)}) collective-permute-start(bf16[1,256]{1,0:T(2,128)(2,1)S(1)} %get-tuple-element.2), channel_id=1, source_target_pairs={{0,4},{4,8},{8,12},{12,16},{16,20},{20,24},{24,28},{28,32},{32,36}... | collective-permute-start | bytes 1544 | tf_op jit(solution)/shard_map/ppermute | solution.py:18
  206.1 4.9 %collective-permute-start.1 = (bf16[1,256]{1,0:T(2,128)(2,1)S(1)}, bf16[1,256]{1,0:T(2,128)(2,1)S(1)}, u32[]{:S(2)}, u32[]{:S(2)}) collective-permute-start(bf16[1,256]{1,0:T(2,128)(2,1)S(1)} %get-tuple-element.3), channel_id=1, source_target_pairs={{4,0},{8,4},{12,8},{16,12},{20,16},{24,20},{28,24},{32,28},{36,32}... | collective-permute-start | bytes 1544 | tf_op jit(solution)/shard_map/ppermute | solution.py:19
  213.3 64.8 %copy-start.6 = (f32[128,2]{0,1:T(2,128)S(1)}, f32[128,2]{0,1:T(2,128)}, u32[]{:S(2)}) copy-start(f32[128,2]{0,1:T(2,128)} %param.20) | copy-start | bytes 3076
  271.3 29.6 %all-to-all-start.1 = ((bf16[16,2,1,12,2048]{4,1,3,2,0:T(2,128)(2,1)}), bf16[16,2,1,12,2048]{4,1,3,2,0:T(2,128)(2,1)S(1)}, u32[]{:S(2)}, u32[]{:S(2)}) async-start(bf16[16,2,1,12,2048]{4,1,3,2,0:T(2,128)(2,1)} %copy.45), calls=%async_computation.3 | async-start | bytes 3145728 | tf_op jit(solution)/shard_map/all_to_all | solution.py:50
Sparse Core Ops, SparseCore 0:
  56.7 62.8 all-gather.2
  201.3 64.7 reduce-scatter.4
  269.1 29.3 reduce-scatter.2
where the time goes:
time: 330 us; the launch traced here: 329 us
  waiting for transfers between devices  141 us (43%)
  local copies, waits for them, and re-layouts  59 us (18%)
  matrix products  50.1 us (15%)
  blocking collectives  45 us (14%)
  between operations  14 us (4%)
  starting transfers between devices  12.6 us (4%)
  other arithmetic  6.86 us (2%)
    all_gather x1, waiting for transfers between devices, on_gathered_pieces(): done.append(jax.vmap(apply)(lax.all_gather(slab, axis), starts))  63 us
    reduce_scatter x1, waiting for transfers between devices, expert_half(): lax.psum_scatter(rounded(jnp.dot(selected, expert_down[0], preferred_elem...  52.8 us
    all_to_all x1, blocking collectives, expert_half(): lax.all_to_all(outgoing, EP, split_axis=0, concat_axis=0, tiled=True)  37.7 us
    all_to_all x1, waiting for transfers between devices, exchange_in_order(): whole = lax.all_to_all(whole, axes[k], k, k, tiled=True)  22.6 us
    dot_general x1, matrix products, hidden_of(): jnp.dot(flat_rows, expert_up[0], preferred_element_type=jnp.float32)  15.7 us
    dot_general x1, matrix products, expert_half(): jnp.dot(selected, expert_down[0], preferred_element_type=jnp.float32)  15.2 us
    dot_general x1, matrix products, hidden_of(): jnp.dot(flat_rows, expert_gate[0], preferred_element_type=jnp.float32)  14.2 us
    reshape x1, local copies, waits for them, and re-layouts, hidden_of(): flat_rows = slot_block.reshape(-1, features)  10.9 us
  transfers between devices with their start and end apart: 6, of which 4 were waited for; matrix products, arithmetic and copies ran while one was open for 7% of the time, Pallas kernels for 0%

commit v1 on v0

v1 whole, which is shorter than its diff:
```python
import functools

import jax
import jax.numpy as jnp
from jax import lax
from jax.experimental import pallas as pl
from jax.experimental.pallas import tpu as pltpu
from jax.sharding import Mesh
from jax.sharding import PartitionSpec as P

EP = ("ep_0", "ep_1", "ep_2")
EP_TP = ("ep_0", "ep_1", "ep_2", "tp")
ZY = ("ep_0", "ep_1")
CHUNKS = ((0, 8), (8, 24))
F32 = jnp.float32
BF16 = jnp.bfloat16


def shift(x, axis, by):
    size = lax.axis_size(axis)
    return lax.ppermute(x, axis, [(i, (i + by) % size) for i in range(size)])


def neighbours(product):
    size = lax.axis_size(EP)
    up = [(i, i + 1) for i in range(size - 1)]
    down = [(j, i) for i, j in up]
    rows = product.shape[0]
    before = lax.ppermute(product[rows - 1 :], EP, up)
    after = lax.ppermute(product[:1], EP, down)
    return before, after


def mixer_rows(value_in, gate_in, outer_gate, conv_weight, out_weight):
    product = (value_in.astype(F32) * gate_in.astype(F32)).astype(BF16)
    before, after = neighbours(product)
    padded = jnp.concatenate([before, product, after], axis=0).astype(F32)
    taps = conv_weight.astype(F32)
    convolved = padded[:-2] * taps[0] + padded[1:-1] * taps[1] + padded[2:] * taps[2]
    mixed_rows = (outer_gate.astype(F32) * convolved).astype(BF16)
    partial = jnp.dot(mixed_rows, out_weight, preferred_element_type=F32).astype(BF16)
    return partial


def mixer_sum(partial):
    tp = lax.axis_size("tp")
    rows, width = partial.shape
    parts = partial.reshape(tp, rows // tp, width)
    parts = lax.all_to_all(parts, "tp", 0, 0, tiled=True)
    return jnp.sum(parts.astype(F32), axis=0).astype(BF16)


def slots_of(routes, core, groups):
    tokens = routes.shape[1]
    mine = (2 * lax.broadcasted_iota(jnp.int32, (groups, tokens), 0) + core).astype(F32)
    match = [jnp.where(routes[k : k + 1] == mine, 1.0, 0.0) for k in range(routes.shape[0])]
    every = sum(match)
    before = lax.broadcasted_iota(jnp.int32, (tokens, tokens), 0)
    after = lax.broadcasted_iota(jnp.int32, (tokens, tokens), 1)
    upper = jnp.where(before < after, 1.0, 0.0).astype(BF16)
    slot = jnp.dot(every.astype(BF16), upper, preferred_element_type=F32)
    return match, every, jnp.where(every > 0.5, slot, -1.0)


def one_hot_rows(value, slot, first, last):
    groups, tokens = slot.shape
    rows = []
    for g in range(groups):
        names = first + lax.broadcasted_iota(jnp.int32, (last - first, tokens), 0)
        rows.append(jnp.where(slot[g : g + 1] == names.astype(F32), value[g : g + 1], 0.0))
    return jnp.concatenate(rows, axis=0)


def dispatch_body(core_ref, own_ref, other_ref, routes_ref, gain_ref, *out_refs):
    groups = 16
    tokens = jnp.concatenate([own_ref[...], other_ref[...]], axis=0).astype(F32)
    scale = lax.rsqrt(jnp.mean(tokens * tokens, axis=-1, keepdims=True) + 1e-06)
    normed = (tokens * scale * gain_ref[...].astype(F32)).astype(BF16)
    _, every, slot = slots_of(routes_ref[...], core_ref[0], groups)
    for (first, last), out_ref in zip(CHUNKS, out_refs):
        hot = one_hot_rows(every, slot, first, last).astype(BF16)
        out_ref[...] = jnp.dot(hot, normed, preferred_element_type=F32).astype(BF16)


def weights_body(core_ref, routes_ref, weight_ref, *out_refs):
    groups = 16
    match, _, slot = slots_of(routes_ref[...], core_ref[0], groups)
    value = sum(m * weight_ref[k : k + 1] for k, m in enumerate(match))
    for (first, last), out_ref in zip(CHUNKS, out_refs):
        hot = one_hot_rows(value, slot, first, last)
        turned = jnp.transpose(hot)
        high = turned.astype(BF16)
        low = (turned - high.astype(F32)).astype(BF16)
        out_ref[0] = high
        out_ref[1] = low


def combine_first_body(weight_ref, rows_ref, out_ref):
    rows = rows_ref[...]
    total = jnp.dot(weight_ref[0], rows, preferred_element_type=F32)
    out_ref[...] = total + jnp.dot(weight_ref[1], rows, preferred_element_type=F32)


def combine_last_body(weight_ref, rows_ref, before_ref, own_ref, other_ref):
    rows = rows_ref[...]
    total = jnp.dot(weight_ref[0], rows, preferred_element_type=F32)
    total = total + jnp.dot(weight_ref[1], rows, preferred_element_type=F32) + before_ref[...]
    half = own_ref.shape[0]
    own_ref[...] = total[:half]
    other_ref[...] = total[half:].astype(BF16)


def small_call(body, outs, *args, scalars=0, name=None):
    specs = [pl.BlockSpec(memory_space=pltpu.SMEM)] * scalars
    specs += [pl.BlockSpec(memory_space=pltpu.VMEM)] * (len(args) - scalars)
    return pl.pallas_call(
        body,
        out_shape=outs,
        in_specs=specs,
        out_specs=jax.tree.map(lambda _: pl.BlockSpec(memory_space=pltpu.VMEM), outs),
        name=name,
        cost_estimate=pl.CostEstimate(flops=2_000_000_000, bytes_accessed=4_000_000, transcendentals=0),
    )(*args)


def ffn_body(*refs, pieces, steps):
    x_refs = refs[:pieces]
    gate_ref, up_ref, down_ref = refs[pieces : pieces + 3]
    out_refs = refs[pieces + 3 : 2 * pieces + 3]
    total_ref = refs[-1]
    step = pl.program_id(0)
    rows = jnp.concatenate([r[...] for r in x_refs], axis=0)
    gate = jnp.dot(rows, gate_ref[0], preferred_element_type=F32)
    up = jnp.dot(rows, up_ref[0], preferred_element_type=F32)
    hidden = (gate / (1.0 + jnp.exp(-gate)) * up).astype(BF16)
    part = jnp.dot(hidden, down_ref[0], preferred_element_type=F32)

    @pl.when(step == 0)
    def _():
        total_ref[...] = part

    @pl.when(jnp.logical_and(step > 0, step < steps - 1))
    def _():
        total_ref[...] += part

    @pl.when(step == steps - 1)
    def _():
        total = (total_ref[...] + part).astype(BF16)
        at = 0
        for out_ref in out_refs:
            count = out_ref.shape[0]
            out_ref[...] = total[at : at + count]
            at += count


def ffn(xs, gate, up, down, name, block=512):
    width, units = gate.shape[1:]
    steps = units // block
    rows = sum(x.shape[0] for x in xs)
    whole = [pl.BlockSpec(x.shape, lambda j: (0, 0)) for x in xs]
    return pl.pallas_call(
        functools.partial(ffn_body, pieces=len(xs), steps=steps),
        grid=(steps,),
        in_specs=whole
        + [
            pl.BlockSpec((1, width, block), lambda j: (0, 0, j)),
            pl.BlockSpec((1, width, block), lambda j: (0, 0, j)),
            pl.BlockSpec((1, block, width), lambda j: (0, j, 0)),
        ],
        out_specs=whole,
        out_shape=[jax.ShapeDtypeStruct(x.shape, BF16) for x in xs],
        scratch_shapes=[pltpu.VMEM((rows, width), F32)],
        compiler_params=pltpu.CompilerParams(vmem_limit_bytes=56 * 1024 * 1024),
        cost_estimate=pl.CostEstimate(
            flops=6 * rows * width * units, bytes_accessed=3 * 2 * width * units, transcendentals=rows * units
        ),
        name=name,
    )(*xs, gate, up, down)


def gather_over_x(x):
    half = x.shape[0] // 2
    left = shift(x, "tp", 1)
    right = shift(x, "tp", -1)
    far_top = shift(left[:half], "tp", 1)
    far_low = shift(right[half:], "tp", -1)
    return left, right, far_top, far_low


def scatter_over_x(own, left, right, far_top, far_low):
    half = far_top.shape[0]
    top = shift(far_top, "tp", 1)
    low = shift(far_low, "tp", -1)
    right_sum = jnp.concatenate([(right[:half].astype(F32) + top.astype(F32)).astype(BF16), right[half:]], axis=0)
    left_sum = jnp.concatenate([left[:half], (left[half:].astype(F32) + low.astype(F32)).astype(BF16)], axis=0)
    from_left = shift(right_sum, "tp", 1)
    from_right = shift(left_sum, "tp", -1)
    return (own.astype(F32) + from_left.astype(F32) + from_right.astype(F32)).astype(BF16)


def over_zy(x):
    count = lax.axis_size(ZY)
    blocks = x.reshape(count, x.shape[0] // count, x.shape[1])
    return lax.all_to_all(blocks, ZY, 0, 0, tiled=True).reshape(x.shape)


def body(
    value_in,
    gate_in,
    outer_gate,
    conv_weight,
    out_weight,
    moe_tokens,
    norm_gain,
    routes,
    route_weight,
    expert_gate,
    expert_up,
    expert_down,
):
    own_rows, width = moe_tokens.shape
    groups = lax.axis_size(ZY)
    core = lax.axis_index("ep_2").astype(jnp.int32).reshape(1)
    facts = jnp.concatenate([routes.T.astype(F32), route_weight.T], axis=0)
    other_facts = shift(facts, "ep_2", 1)
    other_tokens = shift(moe_tokens, "ep_2", 1)
    both = jnp.concatenate([facts, other_facts], axis=1)
    top = routes.shape[1]
    outgoing = small_call(
        dispatch_body,
        [jax.ShapeDtypeStruct((groups * (b - a), width), BF16) for a, b in CHUNKS],
        core,
        moe_tokens,
        other_tokens,
        both[:top],
        norm_gain.reshape(1, width),
        scalars=1,
        name="dispatch",
    )
    arrived = [over_zy(x) for x in outgoing]
    partial = mixer_rows(value_in, gate_in, outer_gate, conv_weight, out_weight)
    mixer_out = mixer_sum(partial)
    weights = small_call(
        weights_body,
        [jax.ShapeDtypeStruct((2, 2 * own_rows, groups * (b - a)), BF16) for a, b in CHUNKS],
        core,
        both[:top],
        both[top:],
        scalars=1,
        name="weights",
    )
    summed = []
    for c, x in enumerate(arrived):
        left, right, far_top, far_low = gather_over_x(x)
        if c == 0:
            parts = ffn([x, left, right, far_top, far_low], expert_gate, expert_up, expert_down, f"ffn_{c}")
        else:
            near = ffn([x, left, right], expert_gate, expert_up, expert_down, f"ffn_near_{c}")
            far = ffn([far_top, far_low], expert_gate, expert_up, expert_down, f"ffn_far_{c}")
            parts = list(near) + list(far)
        summed.append(scatter_over_x(*parts))
    returned = [over_zy(x) for x in summed]
    first = small_call(
        combine_first_body,
        jax.ShapeDtypeStruct((2 * own_rows, width), F32),
        weights[0],
        returned[0],
        name="combine_first",
    )
    own, other = small_call(
        combine_last_body,
        [jax.ShapeDtypeStruct((own_rows, width), F32), jax.ShapeDtypeStruct((own_rows, width), BF16)],
        weights[1],
        returned[1],
        first,
        name="combine_last",
    )
    moe_out = (own + shift(other, "ep_2", 1).astype(F32)).astype(BF16)
    return (mixer_out, moe_out)


def solution(mesh):
    torus = Mesh(mesh.devices.reshape(4, 4, 2, mesh.shape["tp"]), ("ep_0", "ep_1", "ep_2", "tp"))
    placed = (
        P(EP, "tp"),
        P(EP, "tp"),
        P(EP, "tp"),
        P(None, "tp"),
        P("tp", None),
        P(EP_TP, None),
        P(),
        P(EP_TP, None),
        P(EP_TP, None),
        P(EP, None, "tp"),
        P(EP, None, "tp"),
        P(EP, "tp", None),
    )
    return jax.shard_map(
        body,
        mesh=torus,
        in_specs=placed,
        out_specs=(P(EP_TP, None), P(EP_TP, None)),
        check_vma=False,
    )
```

time: 330 us -> 256 us (0.78)
  Pallas kernels: 0 us -> 63.4 us
  waiting for transfers between devices: 141 us -> 80.1 us
  starting transfers between devices: 12.6 us -> 63.5 us
  matrix products: 50.1 us -> 2.15 us
  local copies, waits for them, and re-layouts: 59 us -> 11.9 us
  blocking collectives: 45 us -> 18.5 us
  between operations: 14 us -> 1.04 us
  other arithmetic: 6.86 us -> 12.8 us
    pallas_call x0 -> x7, Pallas kernels: none -> 63.4 us  [the longest x3 51.5 us: ffn(): pl.pallas_call(functools.partial(ffn_body, pieces=len(xs), steps=steps),...]
    all_gather x1 -> x0, waiting for transfers between devices: 63 us -> none  [on_gathered_pieces(): done.append(jax.vmap(apply)(lax.all_gather(slab, axis), starts))]
    ppermute x2 -> x21, waiting for transfers between devices: 2.93 us -> 61.5 us  [the longest x19 57.9 us: shift(): return lax.ppermute(x, axis, [(i, (i + by) % size) for i in range(size)])]
    reduce_scatter x2 -> x0, waiting for transfers between devices: 52.8 us -> none  [the longest x1 52.8 us: expert_half(): lax.psum_scatter(rounded(jnp.dot(selected, expert_down[0], preferred_elem...]
    dot_general x5 -> x1, matrix products: 50.1 us -> 2.15 us  [mixer_rows(): jnp.dot(mixed_rows, out_weight, preferred_element_type=F32).astype(BF16)]
    ppermute x2 -> x21, starting transfers between devices: 5.76 us -> 45.1 us  [the longest x19 24.2 us: shift(): return lax.ppermute(x, axis, [(i, (i + by) % size) for i in range(size)])]
    all_to_all x2 -> x1, blocking collectives: 45 us -> 18.5 us  [over_zy(): return lax.all_to_all(blocks, ZY, 0, 0, tiled=True).reshape(x.shape)]
    reshape x3 -> x1, local copies, waits for them, and re-layouts: 21.5 us -> 1.28 us  [body(): norm_gain.reshape(1, width)]
  transfers between devices with their start and end apart: 6 -> 25, of which waited for: 4 -> 11; matrix products, arithmetic and copies ran while one was open for 7% -> 8% of each run, Pallas kernels for 0% -> 24%
where the time goes in v1:
time: 256 us; the launch traced here: 253 us
  waiting for transfers between devices  80.1 us (31%)
  starting transfers between devices  63.5 us (25%)
  Pallas kernels  63.4 us (25%)
  blocking collectives  18.5 us (7%)
  other arithmetic  12.8 us (5%)
  local copies, waits for them, and re-layouts  11.9 us (5%)
    ppermute x19, waiting for transfers between devices, shift(): return lax.ppermute(x, axis, [(i, (i + by) % size) for i in range(size)])  57.9 us
    pallas_call x3, Pallas kernels, ffn(): pl.pallas_call(functools.partial(ffn_body, pieces=len(xs), steps=steps),...  51.5 us
    ppermute x19, starting transfers between devices, shift(): return lax.ppermute(x, axis, [(i, (i + by) % size) for i in range(size)])  24.2 us
    ppermute x1, starting transfers between devices, neighbours(): before = lax.ppermute(product[rows - 1:], EP, up)  18.9 us
    all_to_all x1, blocking collectives, over_zy(): return lax.all_to_all(blocks, ZY, 0, 0, tiled=True).reshape(x.shape)  18.5 us
    all_to_all x3, starting transfers between devices, over_zy(): return lax.all_to_all(blocks, ZY, 0, 0, tiled=True).reshape(x.shape)  13.8 us
    all_to_all x1, waiting for transfers between devices, mixer_sum(): parts = lax.all_to_all(parts, 'tp', 0, 0, tiled=True)  13.1 us
    pallas_call x4, Pallas kernels, small_call(): pl.pallas_call(body, out_shape=outs, in_specs=specs, out_specs=jax.tree.m...  11.9 us
  transfers between devices with their start and end apart: 25, of which 11 were waited for; matrix products, arithmetic and copies ran while one was open for 8% of the time, Pallas kernels for 24%

profile of v1, /device:TPU:1, one launch (start us, length us, event | category | flops | bytes accessed | tf_op | source)
XLA Modules:
  0.0 253.4 jit_solution(4302725183662889401)
XLA Ops:
  0.6 1.5 collective-permute-start.3
  2.1 0.7 convert_bitcast_fusion
  2.8 0.7 pad_maximum_fusion.5
  3.5 0.1 collective-permute-start.2
  3.6 1.3 reshape.39.gain_ref
  4.8 0.7 pad_maximum_fusion.4
  5.5 0.6 fusion.10
  6.1 0.8 copy-done.18
  6.9 3.2 %dispatch.1 = (bf16[128,2048]{1,0:T(8,128)(2,1)}, bf16[256,2048]{1,0:T(8,128)(2,1)}) custom-call(s32[1]{0:T(128)} %bitcast.4.core_ref, bf16[128,2048]{1,0:T(8,128)(2,1)} %own_ref.1, bf16[128,2048]{1,0:T(8,128)(2,1)} %copy-done.18, f32[2,256]{1,0:T(2,128)} %get-tuple-element.37.routes_ref, bf16[1,2048]{1,0:T(2,128)(2,1)} %reshape.39.gain_ref), custom_call_target="tpu_custom_call" | custom-call | flops 2000000000 | bytes 4000000 | tf_op jit(solution)/shard_map/dispatch/pallas_call | solution.py:116
  10.1 18.5 %all_to_all.25 = bf16[16,8,2048]{2,1,0:T(8,128)(2,1)S(1)} all-to-all(bf16[16,8,2048]{2,1,0:T(8,128)(2,1)} %bitcast.26), channel_id=1, replica_groups=mesh['ep_0'=4,'ep_1'=4,'ep_2'=2,'tp'=4] {'ep_0','ep_1'}, dimensions={0} | all-to-all | bytes 1048576 | tf_op jit(solution)/shard_map/all_to_all | solution.py:204
  28.6 3.7 %all-to-all-start.1 = ((bf16[16,16,2048]{2,1,0:T(8,128)(2,1)}), bf16[16,16,2048]{2,1,0:T(8,128)(2,1)S(1)}, u32[]{:S(2)}, u32[]{:S(2)}) async-start(bf16[16,16,2048]{2,1,0:T(8,128)(2,1)} %bitcast.22), calls=%async_computation.1 | async-start | bytes 2097152 | tf_op jit(solution)/shard_map/all_to_all | solution.py:204
  32.3 1.3 collective-permute-start.12
  33.6 1.5 collective-permute-start.13
  35.1 10.2 %collective-permute-done.12.refs_1_ = bf16[128,2048]{1,0:T(8,128)(2,1)S(1)} collective-permute-done((bf16[128,2048]{1,0:T(8,128)(2,1)S(1)}, bf16[128,2048]{1,0:T(8,128)(2,1)S(1)}, u32[]{:S(2)}, u32[]{:S(2)}) %collective-permute-start.12) | collective-permute-done | bytes 524320 | tf_op jit(solution)/shard_map/ppermute | solution.py:21
  45.4 0.6 copy-done.14
  46.0 0.2 copy-done.15
  46.2 2.6 %collective-permute-start.15 = (bf16[64,2048]{1,0:T(8,128)(2,1)S(1)}, bf16[64,2048]{1,0:T(8,128)(2,1)}, u32[]{:S(2)}, u32[]{:S(2)}) collective-permute-start(bf16[64,2048]{1,0:T(8,128)(2,1)S(1)} %slice.102), channel_id=1, source_target_pairs={{0,3},{1,0},{2,1},{3,2},{4,7},{5,4},{6,5},{7,6},{8,11},{9,8},{10,9... | collective-permute-start | bytes 786440 | tf_op jit(solution)/shard_map/ppermute | solution.py:21
  48.8 2.7 %collective-permute-start.5 = (bf16[256,2048]{1,0:T(8,128)(2,1)S(1)}, bf16[256,2048]{1,0:T(8,128)(2,1)}, u32[]{:S(2)}, u32[]{:S(2)}) collective-permute-start(bf16[256,2048]{1,0:T(8,128)(2,1)S(1)} %bitcast.19), channel_id=1, source_target_pairs={{0,3},{1,0},{2,1},{3,2},{4,7},{5,4},{6,5},{7,6},{8,11},{9,8},{10,9... | collective-permute-start | bytes 3145736 | tf_op jit(solution)/shard_map/ppermute | solution.py:21
  51.5 0.3 collective-permute-done.14.refs_3_
  51.8 0.3 collective-permute-done.15.refs_4_
  52.1 0.4 copy-done.19
  52.5 16.9 %ffn_0.1 = (bf16[128,2048]{1,0:T(8,128)(2,1)}, bf16[128,2048]{1,0:T(8,128)(2,1)}, bf16[128,2048]{1,0:T(8,128)(2,1)}, bf16[64,2048]{1,0:T(8,128)(2,1)}, bf16[64,2048]{1,0:T(8,128)(2,1)}) custom-call(bf16[128,2048]{1,0:T(8,128)(2,1)} %bitcast.25, bf16[128,2048]{1,0:T(8,128)(2,1)} %copy-done.14, bf16[128,2048]{1,0:T(8,128)(2,1)} %copy-done.15, ...), custom_call_target="tpu_custom_call" | custom-call | flops 9663676416 | bytes 18874368 | tf_op jit(solution)/shard_map/ffn_0/pallas_call | solution.py:161
  69.4 0.4 collective-permute-start.16
  69.8 1.0 slice.86
  70.8 2.5 %collective-permute-start.18 = (bf16[64,2048]{1,0:T(8,128)(2,1)}, bf16[64,2048]{1,0:T(8,128)(2,1)S(1)}, u32[]{:S(2)}, u32[]{:S(2)}) collective-permute-start(bf16[64,2048]{1,0:T(8,128)(2,1)} %get-tuple-element.31), channel_id=1, source_target_pairs={{0,3},{1,0},{2,1},{3,2},{4,7},{5,4},{6,5},{7,6},{8,11},{9,8},{10,9... | collective-permute-start | bytes 786440 | tf_op jit(solution)/shard_map/ppermute | solution.py:21
  73.4 1.0 slice.87
  74.3 5.8 %collective-permute-done.16 = bf16[64,2048]{1,0:T(8,128)(2,1)S(1)} collective-permute-done((bf16[64,2048]{1,0:T(8,128)(2,1)}, bf16[64,2048]{1,0:T(8,128)(2,1)S(1)}, u32[]{:S(2)}, u32[]{:S(2)}) %collective-permute-start.16) | collective-permute-done | bytes 262176 | tf_op jit(solution)/shard_map/ppermute | solution.py:21
  80.2 1.0 add_convert_fusion.6
  81.4 1.3 slice.100
  82.7 2.5 collective-permute-start.7
  85.2 0.3 collective-permute-start.17
  85.6 6.6 %collective-permute-done.6.refs_0_ = bf16[128,2048]{1,0:T(8,128)(2,1)S(1)} collective-permute-done((bf16[128,2048]{1,0:T(8,128)(2,1)S(1)}, bf16[128,2048]{1,0:T(8,128)(2,1)S(1)}, u32[]{:S(2)}, u32[]{:S(2)}) %collective-permute-start.6) | collective-permute-done | bytes 524320 | tf_op jit(solution)/shard_map/ppermute | solution.py:21
  92.2 0.2 collective-permute-done.7.refs_1_
  92.4 0.6 copy-done.5
  93.0 0.8 copy-done.6
  93.8 11.7 %ffn_far_1.1 = (bf16[128,2048]{1,0:T(8,128)(2,1)}, bf16[128,2048]{1,0:T(8,128)(2,1)}) custom-call(bf16[128,2048]{1,0:T(8,128)(2,1)} %copy-done.5, bf16[128,2048]{1,0:T(8,128)(2,1)} %copy-done.6, bf16[1,2048,1536]{2,1,0:T(8,128)(2,1)} %refs_5_.3, bf16[1,2048,1536]{2,1,0:T(8,128)(2,1)} %refs_6_.1, bf16[1,1536,2048]{2,1,0:T(8,128)(2,1)} %refs_7_.1), custom_call_target="tpu_custom_call" | custom-call | flops 4831838208 | bytes 18874368 | tf_op jit(solution)/shard_map/ffn_far_1/pallas_call | solution.py:161
  105.5 22.9 %ffn_near_1.1 = (bf16[256,2048]{1,0:T(8,128)(2,1)}, bf16[256,2048]{1,0:T(8,128)(2,1)}, bf16[256,2048]{1,0:T(8,128)(2,1)}) custom-call(bf16[256,2048]{1,0:T(8,128)(2,1)} %bitcast.20, bf16[256,2048]{1,0:T(8,128)(2,1)} %copy-done.13, bf16[256,2048]{1,0:T(8,128)(2,1)} %collective-permute-done.5.refs_2_, bf16[1,2048,1536]{2,1,0:T(8,128)(2,1)} %refs_5_.3, ...), custom_call_target="tpu_custom_call" | custom-call | flops 14495514624 | bytes 18874368 | tf_op jit(solution)/shard_map/ffn_near_1/pallas_call | solution.py:161
  128.4 1.2 slice.80
  129.6 1.1 slice.81
  130.7 2.8 %collective-permute-start.10 = (bf16[128,2048]{1,0:T(8,128)(2,1)S(1)}, bf16[128,2048]{1,0:T(8,128)(2,1)S(1)}, u32[]{:S(2)}, u32[]{:S(2)}) collective-permute-start(bf16[128,2048]{1,0:T(8,128)(2,1)S(1)} %copy-done.17), channel_id=1, source_target_pairs={{0,3},{1,0},{2,1},{3,2},{4,7},{5,4},{6,5},{7,6},{8,11},{9,8},{10,9... | collective-permute-start | bytes 1572872 | tf_op jit(solution)/shard_map/ppermute | solution.py:21
  133.5 0.1 add_convert_fusion.4
  133.8 5.8 %collective-permute-done.10 = bf16[128,2048]{1,0:T(8,128)(2,1)S(1)} collective-permute-done((bf16[128,2048]{1,0:T(8,128)(2,1)S(1)}, bf16[128,2048]{1,0:T(8,128)(2,1)S(1)}, u32[]{:S(2)}, u32[]{:S(2)}) %collective-permute-start.10) | collective-permute-done | bytes 524320 | tf_op jit(solution)/shard_map/ppermute | solution.py:21
  139.7 0.1 add_convert_fusion.3
  139.9 3.2 %collective-permute-start.11 = (bf16[256,2048]{1,0:T(8,128)(2,1)S(1)}, bf16[256,2048]{1,0:T(8,128)(2,1)}, u32[]{:S(2)}, u32[]{:S(2)}) collective-permute-start(bf16[256,2048]{1,0:T(8,128)(2,1)S(1)} %pad_maximum_fusion.1), channel_id=1, source_target_pairs={{0,3},{1,0},{2,1},{3,2},{4,7},{5,4},{6,5},{7,6},{8,11},{9,8},{10,9... | collective-permute-start | bytes 3145736 | tf_op jit(solution)/shard_map/ppermute | solution.py:21
  143.1 0.3 collective-permute-start.19
  143.4 28.6 %collective-permute-done.19 = bf16[128,2048]{1,0:T(8,128)(2,1)S(1)} collective-permute-done((bf16[128,2048]{1,0:T(8,128)(2,1)S(1)}, bf16[128,2048]{1,0:T(8,128)(2,1)S(1)}, u32[]{:S(2)}, u32[]{:S(2)}) %collective-permute-start.19) | collective-permute-done | bytes 524320 | tf_op jit(solution)/shard_map/ppermute | solution.py:21
  172.0 2.1 fusion
  174.1 6.4 %all-to-all-start.4 = ((bf16[16,8,2048]{2,1,0:T(8,128)(2,1)}), bf16[16,8,2048]{2,1,0:T(8,128)(2,1)}, u32[]{:S(2)}, u32[]{:S(2)}) async-start(bf16[16,8,2048]{2,1,0:T(8,128)(2,1)} %fusion), calls=%async_computation.4 | async-start | bytes 1048576 | tf_op jit(solution)/shard_map/all_to_all | solution.py:204
  180.6 3.4 %add_convert_fusion = bf16[256,2048]{1,0:T(8,128)(2,1)} fusion(bf16[256,2048]{1,0:T(8,128)(2,1)} %collective-permute-done.11, bf16[256,2048]{1,0:T(8,128)(2,1)} %collective-permute-done.9, bf16[256,2048]{1,0:T(8,128)(2,1)} %get-tuple-element.20), kind=kLoop, calls=%fused_computation.1 | loop fusion | flops 3145728 | bytes 4194304 | tf_op jit(solution)/shard_map/convert_element_type | solution.py:198
  184.0 5.6 %all-to-all-done.4 = bf16[16,8,2048]{2,1,0:T(8,128)(2,1)} async-done(((bf16[16,8,2048]{2,1,0:T(8,128)(2,1)}), bf16[16,8,2048]{2,1,0:T(8,128)(2,1)}, u32[]{:S(2)}, u32[]{:S(2)}) %all-to-all-start.4) | async-done | bytes 524320 | tf_op jit(solution)/shard_map/all_to_all | solution.py:204
  189.6 3.7 %all-to-all-start.2 = ((bf16[16,16,2048]{2,1,0:T(8,128)(2,1)}), bf16[16,16,2048]{2,1,0:T(8,128)(2,1)S(1)}, u32[]{:S(2)}, u32[]{:S(2)}) async-start(bf16[16,16,2048]{2,1,0:T(8,128)(2,1)} %bitcast.9), calls=%async_computation.2 | async-start | bytes 2097152 | tf_op jit(solution)/shard_map/all_to_all | solution.py:204
  193.4 18.9 %collective-permute-start = (bf16[1,256]{1,0:T(2,128)(2,1)S(1)}, bf16[1,256]{1,0:T(2,128)(2,1)S(1)}, u32[]{:S(2)}, u32[]{:S(2)}) collective-permute-start(bf16[1,256]{1,0:T(2,128)(2,1)S(1)} %get-tuple-element.34), channel_id=1, source_target_pairs={{0,4},{4,8},{8,12},{12,16},{16,20},{20,24},{24,28},{28,32},{32,36}... | collective-permute-start | bytes 1544 | tf_op jit(solution)/shard_map/ppermute | solution.py:29
  212.3 1.9 collective-permute-start.1
  214.3 3.5 %collective-permute-done.1 = bf16[1,256]{1,0:T(2,128)(2,1)S(1)} collective-permute-done((bf16[1,256]{1,0:T(2,128)(2,1)S(1)}, bf16[1,256]{1,0:T(2,128)(2,1)S(1)}, u32[]{:S(2)}, u32[]{:S(2)}) %collective-permute-start.1) | collective-permute-done | bytes 544 | tf_op jit(solution)/shard_map/ppermute | solution.py:30
  217.9 2.2 convolution_convert_fusion
  220.0 1.0 copy-done.4
  221.0 4.7 %all-to-all-start = ((bf16[4,128,2048]{2,1,0:T(8,128)(2,1)}), bf16[4,128,2048]{2,1,0:T(8,128)(2,1)S(1)}, u32[]{:S(2)}, u32[]{:S(2)}) async-start(bf16[4,128,2048]{2,1,0:T(8,128)(2,1)} %bitcast.3), calls=%async_computation | async-start | bytes 4194304 | tf_op jit(solution)/shard_map/all_to_all | solution.py:49
  225.7 1.7 weights.1
  227.4 3.2 %combine_first.1.before_ref = f32[256,2048]{1,0:T(8,128)} custom-call(bf16[2,256,128]{2,1,0:T(8,128)(2,1)} %get-tuple-element.25.weight_ref, bf16[128,2048]{1,0:T(8,128)(2,1)} %bitcast.14.rows_ref), custom_call_target="tpu_custom_call" | custom-call | flops 2000000000 | bytes 4000000 | tf_op jit(solution)/shard_map/combine_first/pallas_call | solution.py:116
  230.6 3.8 %combine_last.1 = (f32[128,2048]{1,0:T(8,128)}, bf16[128,2048]{1,0:T(8,128)(2,1)}) custom-call(bf16[2,256,256]{2,1,0:T(8,128)(2,1)} %get-tuple-element.18.weight_ref, bf16[256,2048]{1,0:T(8,128)(2,1)} %bitcast.21, f32[256,2048]{1,0:T(8,128)} %combine_first.1.before_ref), custom_call_target="tpu_custom_call" | custom-call | flops 2000000000 | bytes 4000000 | tf_op jit(solution)/shard_map/combine_last/pallas_call | solution.py:116
  234.4 2.4 collective-permute-start.20
  236.7 13.1 %all-to-all-done = bf16[4,128,2048]{2,1,0:T(8,128)(2,1)S(1)} async-done(((bf16[4,128,2048]{2,1,0:T(8,128)(2,1)}), bf16[4,128,2048]{2,1,0:T(8,128)(2,1)S(1)}, u32[]{:S(2)}, u32[]{:S(2)}) %all-to-all-start) | async-done | bytes 2097184 | tf_op jit(solution)/shard_map/all_to_all | solution.py:49
  249.8 1.3 reduce_sum.12
  251.1 2.3 add_convert_fusion.1
  (64 shorter events, 0.8 us)
Async XLA Ops:
  0.6 217.2 %copy-start = (bf16[256,2048]{1,0:T(8,128)(2,1)S(1)}, bf16[256,2048]{1,0:T(8,128)(2,1)}, u32[]{:S(2)}) copy-start(bf16[256,2048]{1,0:T(8,128)(2,1)} %param.16) | copy-start | bytes 3145732
  0.6 5.5 %collective-permute-start.3 = (bf16[128,2048]{1,0:T(8,128)(2,1)}, bf16[128,2048]{1,0:T(8,128)(2,1)S(1)}, u32[]{:S(2)}, u32[]{:S(2)}) collective-permute-start(bf16[128,2048]{1,0:T(8,128)(2,1)} %own_ref.1), channel_id=1, source_target_pairs={{0,4},{4,0},{1,5},{5,1},{2,6},{6,2},{3,7},{7,3},{8,12},{12,8},{9,1... | collective-permute-start | bytes 1572872 | tf_op jit(solution)/shard_map/ppermute | solution.py:21
  3.5 1.4 collective-permute-start.2
  6.1 0.8 copy-start.18
  28.6 23.5 %copy-start.8 = (bf16[16,8,2048]{2,1,0:T(8,128)(2,1)}, bf16[16,8,2048]{2,1,0:T(8,128)(2,1)S(1)}, u32[]{:S(2)}) copy-start(bf16[16,8,2048]{2,1,0:T(8,128)(2,1)S(1)} %all_to_all.25) | copy-start | bytes 1572868
  28.6 20.2 %all-to-all-start.1 = ((bf16[16,16,2048]{2,1,0:T(8,128)(2,1)}), bf16[16,16,2048]{2,1,0:T(8,128)(2,1)S(1)}, u32[]{:S(2)}, u32[]{:S(2)}) async-start(bf16[16,16,2048]{2,1,0:T(8,128)(2,1)} %bitcast.22), calls=%async_computation.1 | async-start | bytes 2097152 | tf_op jit(solution)/shard_map/all_to_all | solution.py:204
  32.3 12.9 %collective-permute-start.12 = (bf16[128,2048]{1,0:T(8,128)(2,1)S(1)}, bf16[128,2048]{1,0:T(8,128)(2,1)S(1)}, u32[]{:S(2)}, u32[]{:S(2)}) collective-permute-start(bf16[128,2048]{1,0:T(8,128)(2,1)S(1)} %bitcast.23), channel_id=1, source_target_pairs={{0,1},{1,2},{2,3},{3,0},{4,5},{5,6},{6,7},{7,4},{8,9},{9,10},{10,1... | collective-permute-start | bytes 1572872 | tf_op jit(solution)/shard_map/ppermute | solution.py:21
  33.6 11.8 %collective-permute-start.13 = (bf16[128,2048]{1,0:T(8,128)(2,1)S(1)}, bf16[128,2048]{1,0:T(8,128)(2,1)S(1)}, u32[]{:S(2)}, u32[]{:S(2)}) collective-permute-start(bf16[128,2048]{1,0:T(8,128)(2,1)S(1)} %bitcast.24), channel_id=1, source_target_pairs={{0,3},{1,0},{2,1},{3,2},{4,7},{5,4},{6,5},{7,6},{8,11},{9,8},{10,9... | collective-permute-start | bytes 1572872 | tf_op jit(solution)/shard_map/ppermute | solution.py:21
  45.2 0.8 copy-start.14
  45.3 6.5 %collective-permute-start.14 = (bf16[64,2048]{1,0:T(8,128)(2,1)S(1)}, bf16[64,2048]{1,0:T(8,128)(2,1)S(1)}, u32[]{:S(2)}, u32[]{:S(2)}) collective-permute-start(bf16[64,2048]{1,0:T(8,128)(2,1)S(1)} %slice.101), channel_id=1, source_target_pairs={{0,1},{1,2},{2,3},{3,0},{4,5},{5,6},{6,7},{7,4},{8,9},{9,10},{10,1... | collective-permute-start | bytes 786440 | tf_op jit(solution)/shard_map/ppermute | solution.py:21
  45.4 0.8 copy-start.15
  46.2 5.9 %collective-permute-start.15 = (bf16[64,2048]{1,0:T(8,128)(2,1)S(1)}, bf16[64,2048]{1,0:T(8,128)(2,1)}, u32[]{:S(2)}, u32[]{:S(2)}) collective-permute-start(bf16[64,2048]{1,0:T(8,128)(2,1)S(1)} %slice.102), channel_id=1, source_target_pairs={{0,3},{1,0},{2,1},{3,2},{4,7},{5,4},{6,5},{7,6},{8,11},{9,8},{10,9... | collective-permute-start | bytes 786440 | tf_op jit(solution)/shard_map/ppermute | solution.py:21
  48.8 20.6 %copy-start.3 = (bf16[16,16,2048]{2,1,0:T(8,128)(2,1)}, bf16[16,16,2048]{2,1,0:T(8,128)(2,1)S(1)}, u32[]{:S(2)}) copy-start(bf16[16,16,2048]{2,1,0:T(8,128)(2,1)S(1)} %all-to-all-done.1) | copy-start | bytes 3145732
  48.8 32.4 %collective-permute-start.4 = (bf16[256,2048]{1,0:T(8,128)(2,1)S(1)}, bf16[256,2048]{1,0:T(8,128)(2,1)S(1)}, u32[]{:S(2)}, u32[]{:S(2)}) collective-permute-start(bf16[256,2048]{1,0:T(8,128)(2,1)S(1)} %bitcast.18), channel_id=1, source_target_pairs={{0,1},{1,2},{2,3},{3,0},{4,5},{5,6},{6,7},{7,4},{8,9},{9,10},{10,1... | collective-permute-start | bytes 3145736 | tf_op jit(solution)/shard_map/ppermute | solution.py:21
  48.8 32.5 %collective-permute-start.5 = (bf16[256,2048]{1,0:T(8,128)(2,1)S(1)}, bf16[256,2048]{1,0:T(8,128)(2,1)}, u32[]{:S(2)}, u32[]{:S(2)}) collective-permute-start(bf16[256,2048]{1,0:T(8,128)(2,1)S(1)} %bitcast.19), channel_id=1, source_target_pairs={{0,3},{1,0},{2,1},{3,2},{4,7},{5,4},{6,5},{7,6},{8,11},{9,8},{10,9... | collective-permute-start | bytes 3145736 | tf_op jit(solution)/shard_map/ppermute | solution.py:21
  51.8 0.7 copy-start.19
  69.4 10.8 %collective-permute-start.16 = (bf16[64,2048]{1,0:T(8,128)(2,1)}, bf16[64,2048]{1,0:T(8,128)(2,1)S(1)}, u32[]{:S(2)}, u32[]{:S(2)}) collective-permute-start(bf16[64,2048]{1,0:T(8,128)(2,1)} %get-tuple-element.29), channel_id=1, source_target_pairs={{0,1},{1,2},{2,3},{3,0},{4,5},{5,6},{6,7},{7,4},{8,9},{9,10},{10,1... | collective-permute-start | bytes 786440 | tf_op jit(solution)/shard_map/ppermute | solution.py:21
  70.8 14.7 %collective-permute-start.18 = (bf16[64,2048]{1,0:T(8,128)(2,1)}, bf16[64,2048]{1,0:T(8,128)(2,1)S(1)}, u32[]{:S(2)}, u32[]{:S(2)}) collective-permute-start(bf16[64,2048]{1,0:T(8,128)(2,1)} %get-tuple-element.31), channel_id=1, source_target_pairs={{0,3},{1,0},{2,1},{3,2},{4,7},{5,4},{6,5},{7,6},{8,11},{9,8},{10,9... | collective-permute-start | bytes 786440 | tf_op jit(solution)/shard_map/ppermute | solution.py:21
  74.3 11.2 %copy-start.7 = (bf16[128,2048]{1,0:T(8,128)(2,1)S(1)}, bf16[128,2048]{1,0:T(8,128)(2,1)}, u32[]{:S(2)}) copy-start(bf16[128,2048]{1,0:T(8,128)(2,1)} %get-tuple-element.30) | copy-start | bytes 1572868
  81.2 1.5 copy-start.13
  81.3 10.9 %collective-permute-start.6 = (bf16[128,2048]{1,0:T(8,128)(2,1)S(1)}, bf16[128,2048]{1,0:T(8,128)(2,1)S(1)}, u32[]{:S(2)}, u32[]{:S(2)}) collective-permute-start(bf16[128,2048]{1,0:T(8,128)(2,1)S(1)} %slice.99), channel_id=1, source_target_pairs={{0,1},{1,2},{2,3},{3,0},{4,5},{5,6},{6,7},{7,4},{8,9},{9,10},{10,1... | collective-permute-start | bytes 1572872 | tf_op jit(solution)/shard_map/ppermute | solution.py:21
  82.7 9.7 %collective-permute-start.7 = (bf16[128,2048]{1,0:T(8,128)(2,1)S(1)}, bf16[128,2048]{1,0:T(8,128)(2,1)S(1)}, u32[]{:S(2)}, u32[]{:S(2)}) collective-permute-start(bf16[128,2048]{1,0:T(8,128)(2,1)S(1)} %slice.100), channel_id=1, source_target_pairs={{0,3},{1,0},{2,1},{3,2},{4,7},{5,4},{6,5},{7,6},{8,11},{9,8},{10,9... | collective-permute-start | bytes 1572872 | tf_op jit(solution)/shard_map/ppermute | solution.py:21
  85.2 58.2 %collective-permute-start.17 = (bf16[128,2048]{1,0:T(8,128)(2,1)S(1)}, bf16[128,2048]{1,0:T(8,128)(2,1)}, u32[]{:S(2)}, u32[]{:S(2)}) collective-permute-start(bf16[128,2048]{1,0:T(8,128)(2,1)S(1)} %pad_maximum_fusion.2), channel_id=1, source_target_pairs={{0,1},{1,2},{2,3},{3,0},{4,5},{5,6},{6,7},{7,4},{8,9},{9,10},{10,1... | collective-permute-start | bytes 1572872 | tf_op jit(solution)/shard_map/ppermute | solution.py:21
  92.2 0.8 copy-start.5
  93.0 0.8 copy-start.6
  105.5 28.1 %collective-permute-start.8 = (bf16[128,2048]{1,0:T(8,128)(2,1)}, bf16[128,2048]{1,0:T(8,128)(2,1)S(1)}, u32[]{:S(2)}, u32[]{:S(2)}) collective-permute-start(bf16[128,2048]{1,0:T(8,128)(2,1)} %get-tuple-element.22), channel_id=1, source_target_pairs={{0,1},{1,2},{2,3},{3,0},{4,5},{5,6},{6,7},{7,4},{8,9},{9,10},{10,1... | collective-permute-start | bytes 1572872 | tf_op jit(solution)/shard_map/ppermute | solution.py:21
  128.4 2.3 copy-start.17
  128.4 5.2 %copy-start.2 = (bf16[256,2048]{1,0:T(8,128)(2,1)S(1)}, bf16[256,2048]{1,0:T(8,128)(2,1)}, u32[]{:S(2)}) copy-start(bf16[256,2048]{1,0:T(8,128)(2,1)} %get-tuple-element.21) | copy-start | bytes 3145732
  130.7 9.0 %copy-start.1 = (bf16[256,2048]{1,0:T(8,128)(2,1)S(1)}, bf16[256,2048]{1,0:T(8,128)(2,1)}, u32[]{:S(2)}) copy-start(bf16[256,2048]{1,0:T(8,128)(2,1)} %get-tuple-element.23) | copy-start | bytes 3145732
  130.7 9.0 %collective-permute-start.10 = (bf16[128,2048]{1,0:T(8,128)(2,1)S(1)}, bf16[128,2048]{1,0:T(8,128)(2,1)S(1)}, u32[]{:S(2)}, u32[]{:S(2)}) collective-permute-start(bf16[128,2048]{1,0:T(8,128)(2,1)S(1)} %copy-done.17), channel_id=1, source_target_pairs={{0,3},{1,0},{2,1},{3,2},{4,7},{5,4},{6,5},{7,6},{8,11},{9,8},{10,9... | collective-permute-start | bytes 1572872 | tf_op jit(solution)/shard_map/ppermute | solution.py:21
  133.7 38.3 %copy-start.9 = (bf16[128,2048]{1,0:T(8,128)(2,1)S(1)}, bf16[128,2048]{1,0:T(8,128)(2,1)}, u32[]{:S(2)}) copy-start(bf16[128,2048]{1,0:T(8,128)(2,1)} %get-tuple-element.27) | copy-start | bytes 1572868
  133.8 46.8 %collective-permute-start.9 = (bf16[256,2048]{1,0:T(8,128)(2,1)S(1)}, bf16[256,2048]{1,0:T(8,128)(2,1)}, u32[]{:S(2)}, u32[]{:S(2)}) collective-permute-start(bf16[256,2048]{1,0:T(8,128)(2,1)S(1)} %pad_maximum_fusion), channel_id=1, source_target_pairs={{0,1},{1,2},{2,3},{3,0},{4,5},{5,6},{6,7},{7,4},{8,9},{9,10},{10,1... | collective-permute-start | bytes 3145736 | tf_op jit(solution)/shard_map/ppermute | solution.py:21
  139.9 40.7 %collective-permute-start.11 = (bf16[256,2048]{1,0:T(8,128)(2,1)S(1)}, bf16[256,2048]{1,0:T(8,128)(2,1)}, u32[]{:S(2)}, u32[]{:S(2)}) collective-permute-start(bf16[256,2048]{1,0:T(8,128)(2,1)S(1)} %pad_maximum_fusion.1), channel_id=1, source_target_pairs={{0,3},{1,0},{2,1},{3,2},{4,7},{5,4},{6,5},{7,6},{8,11},{9,8},{10,9... | collective-permute-start | bytes 3145736 | tf_op jit(solution)/shard_map/ppermute | solution.py:21
  143.1 28.9 %collective-permute-start.19 = (bf16[128,2048]{1,0:T(8,128)(2,1)S(1)}, bf16[128,2048]{1,0:T(8,128)(2,1)S(1)}, u32[]{:S(2)}, u32[]{:S(2)}) collective-permute-start(bf16[128,2048]{1,0:T(8,128)(2,1)S(1)} %pad_maximum_fusion.3), channel_id=1, source_target_pairs={{0,3},{1,0},{2,1},{3,2},{4,7},{5,4},{6,5},{7,6},{8,11},{9,8},{10,9... | collective-permute-start | bytes 1572872 | tf_op jit(solution)/shard_map/ppermute | solution.py:21
  174.1 15.5 %all-to-all-start.4 = ((bf16[16,8,2048]{2,1,0:T(8,128)(2,1)}), bf16[16,8,2048]{2,1,0:T(8,128)(2,1)}, u32[]{:S(2)}, u32[]{:S(2)}) async-start(bf16[16,8,2048]{2,1,0:T(8,128)(2,1)} %fusion), calls=%async_computation.4 | async-start | bytes 1048576 | tf_op jit(solution)/shard_map/all_to_all | solution.py:204
  184.0 9.3 %copy-start.10 = (bf16[512,256]{1,0:T(8,128)(2,1)S(1)}, bf16[512,256]{1,0:T(8,128)(2,1)}, u32[]{:S(2)}) copy-start(bf16[512,256]{1,0:T(8,128)(2,1)} %param.13) | copy-start | bytes 786436
  184.0 9.3 %copy-start.11 = (bf16[512,256]{1,0:T(8,128)(2,1)S(1)}, bf16[512,256]{1,0:T(8,128)(2,1)}, u32[]{:S(2)}) copy-start(bf16[512,256]{1,0:T(8,128)(2,1)} %param.12) | copy-start | bytes 786436
  184.0 30.2 %copy-start.16 = (bf16[3,256]{1,0:T(4,128)(2,1)S(1)}, bf16[3,256]{1,0:T(4,128)(2,1)}, u32[]{:S(2)}) copy-start(bf16[3,256]{1,0:T(4,128)(2,1)} %param.15) | copy-start | bytes 4612
  184.0 33.8 %copy-start.12 = (bf16[512,256]{1,0:T(8,128)(2,1)S(1)}, bf16[512,256]{1,0:T(8,128)(2,1)}, u32[]{:S(2)}) copy-start(bf16[512,256]{1,0:T(8,128)(2,1)} %param.14) | copy-start | bytes 786436
  189.6 30.4 %all-to-all-start.2 = ((bf16[16,16,2048]{2,1,0:T(8,128)(2,1)}), bf16[16,16,2048]{2,1,0:T(8,128)(2,1)S(1)}, u32[]{:S(2)}, u32[]{:S(2)}) async-start(bf16[16,16,2048]{2,1,0:T(8,128)(2,1)} %bitcast.9), calls=%async_computation.2 | async-start | bytes 2097152 | tf_op jit(solution)/shard_map/all_to_all | solution.py:204
  193.4 20.9 %collective-permute-start = (bf16[1,256]{1,0:T(2,128)(2,1)S(1)}, bf16[1,256]{1,0:T(2,128)(2,1)S(1)}, u32[]{:S(2)}, u32[]{:S(2)}) collective-permute-start(bf16[1,256]{1,0:T(2,128)(2,1)S(1)} %get-tuple-element.34), channel_id=1, source_target_pairs={{0,4},{4,8},{8,12},{12,16},{16,20},{20,24},{24,28},{28,32},{32,36}... | collective-permute-start | bytes 1544 | tf_op jit(solution)/shard_map/ppermute | solution.py:29
  212.3 5.5 %collective-permute-start.1 = (bf16[1,256]{1,0:T(2,128)(2,1)S(1)}, bf16[1,256]{1,0:T(2,128)(2,1)S(1)}, u32[]{:S(2)}, u32[]{:S(2)}) collective-permute-start(bf16[1,256]{1,0:T(2,128)(2,1)S(1)} %get-tuple-element.35), channel_id=1, source_target_pairs={{4,0},{8,4},{12,8},{16,12},{20,16},{24,20},{28,24},{32,28},{36,32}... | collective-permute-start | bytes 1544 | tf_op jit(solution)/shard_map/ppermute | solution.py:30
  220.0 1.0 copy-start.4
  221.0 28.8 %all-to-all-start = ((bf16[4,128,2048]{2,1,0:T(8,128)(2,1)}), bf16[4,128,2048]{2,1,0:T(8,128)(2,1)S(1)}, u32[]{:S(2)}, u32[]{:S(2)}) async-start(bf16[4,128,2048]{2,1,0:T(8,128)(2,1)} %bitcast.3), calls=%async_computation | async-start | bytes 4194304 | tf_op jit(solution)/shard_map/all_to_all | solution.py:49
  234.4 16.7 %collective-permute-start.20 = (bf16[128,2048]{1,0:T(8,128)(2,1)}, bf16[128,2048]{1,0:T(8,128)(2,1)}, u32[]{:S(2)}, u32[]{:S(2)}) collective-permute-start(bf16[128,2048]{1,0:T(8,128)(2,1)} %get-tuple-element.33), channel_id=1, source_target_pairs={{0,4},{4,0},{1,5},{5,1},{2,6},{6,2},{3,7},{7,3},{8,12},{12,8},{9,1... | collective-permute-start | bytes 1572872 | tf_op jit(solution)/shard_map/ppermute | solution.py:21
